TPU v7x, 32 devices: a whole 2x2x4 slice. The times are simulated.
32 devices in a mesh: sp: 8 (over z, x), tp: 4 (over y, core).
Axes of the slice: x: 2, y: 2, z: 4, core: 2. Of those that a mesh axis runs over, the one named last changes fastest.
Arguments:
- residual: bfloat16 [4096, 2048], P(('sp', 'tp')), may hold values from -6 to 6
- conv_value: bfloat16 [4096, 1024], P('sp', 'tp'), may hold values from -6 to 6
- conv_gate: bfloat16 [4096, 1024], P('sp', 'tp'), may hold values from -9 to 9
- segments: int32 [4096], P('sp'), may hold values from 0 to 3, never falling along the last dimension, each value on 1 to 2048 neighbouring positions
- conv_weight: float32 [31, 1024], P(None, 'tp'), may hold values from -1 to 1
- norm_gain: float32 [1024], P('tp'), may hold values from 0.1 to 1.9
- norm_shift: float32 [1024], P('tp'), may hold values from -3 to 3
- out_weight: bfloat16 [1024, 2048], replicated, may hold values from -0.1875 to 0.1875
- ffn_gain: float32 [2048], replicated, may hold values from 0.1 to 1.9
- routes: int32 [4096, 2], P('sp'), may hold values from 0 to 7, all different within a row; in each aligned block of 128 rows (0 to 127, 128 to 255, ...) at most 64 rows name the same one
- route_weights: float32 [4096, 2], P('sp'), may hold values from 0.2 to 1
- w_gate: bfloat16 [8, 2048, 1024], P('sp', None, 'tp'), may hold values from -0.125 to 0.125
- w_up: bfloat16 [8, 2048, 1024], P('sp', None, 'tp'), may hold values from -0.125 to 0.125
- w_down: bfloat16 [8, 1024, 2048], P('sp', 'tp'), may hold values from -0.1875 to 0.1875
Outputs:
- layer_out: bfloat16 [4096, 2048], P(('sp', 'tp'))
Inputs may be any that keep to these rules, and one draw needn't show every extreme that they name: `routes`: within the rows of one device (aligned blocks of 512 / 4 rows), no expert is named more than 64 times; the two experts of a row differ. `segments`: document numbers never fall along the sequence.
All inputs are finite; a program needn't handle non-finite values.
Results may differ from a plain program's by a relative error of at most 0.007.
Values may be sent and summed in bfloat16 or wider, within the bound.
A program may use at most 128 MiB of HBM per device.

v0:
```python
import jax
import jax.numpy as jnp
from jax import lax
from jax.sharding import PartitionSpec as P

DC = 1024
CONV_GROUPS = 8


def passed_along(value, axis, steps):
    count = lax.axis_size(axis)
    initial, last = (max(0, -steps), min(count, count - steps))
    return lax.ppermute(value, axis, [(source, source + steps) for source in range(initial, last)])


def slot_numbers(block_routes, capacity, experts_n):
    route_pairs = block_routes.reshape(block_routes.shape[:-2] + (-1,))
    onehot = (route_pairs[..., None] == jnp.arange(experts_n, dtype=jnp.int32)).astype(jnp.int32)
    slot_rank = jnp.sum((jnp.cumsum(onehot, axis=-2) - onehot) * onehot, axis=-1)
    return (route_pairs * capacity + slot_rank).reshape(block_routes.shape)


def dispatch_matrix(slot_ids, slot_total):
    numbers = jnp.arange(slot_total, dtype=jnp.int32)[:, None, None]
    matches = jnp.any(numbers == slot_ids[..., None, :, :], axis=-1)
    return matches.astype(jnp.bfloat16)


def shards(
    residual,
    conv_value,
    conv_gate,
    segments,
    conv_weight,
    norm_gain,
    norm_shift,
    out_weight,
    ffn_gain,
    routes,
    route_weights,
    w_gate,
    w_up,
    w_down,
):
    tok_dev, local_channels = conv_value.shape
    reach = conv_weight.shape[0] - 1
    whole_gate, whole_up = (
        lax.all_gather(w_gate[0], "tp", axis=1, tiled=True),
        lax.all_gather(w_up[0], "tp", axis=1, tiled=True),
    )
    whole_down = lax.all_gather(w_down[0], "tp", axis=0, tiled=True)
    gated = (conv_value.astype(jnp.float32) * jax.nn.sigmoid(conv_gate.astype(jnp.float32))).astype(
        jnp.bfloat16
    )
    rim_prev, seg_prev = passed_along(
        (gated[tok_dev - reach :], segments[tok_dev - reach :]), "sp", 1
    )
    extended = jnp.concatenate([rim_prev, gated], 0).astype(jnp.float32)
    seg_ext = jnp.concatenate([seg_prev, segments], 0)
    convolved = jnp.zeros((tok_dev, local_channels), jnp.float32)
    for offset in range(reach + 1):
        same_doc = (seg_ext[offset : offset + tok_dev] == segments)[:, None]
        convolved = convolved + jnp.where(
            same_doc, extended[offset : offset + tok_dev] * conv_weight[offset], 0.0
        )
    group_size = DC // CONV_GROUPS
    grouped = convolved.reshape(tok_dev, local_channels // group_size, group_size)
    group_mean = jnp.mean(grouped, axis=-1, keepdims=True)
    group_var = jnp.mean(jnp.square(grouped - group_mean), axis=-1, keepdims=True)
    scaled = ((grouped - group_mean) * lax.rsqrt(group_var + 1e-05)).reshape(
        tok_dev, local_channels
    ) * norm_gain + norm_shift
    conv_out = jax.nn.silu(scaled).astype(jnp.bfloat16)
    columns = lax.axis_size("tp")
    column = lax.axis_index("tp")
    rows_own = tok_dev // columns
    weight_rows = lax.dynamic_slice_in_dim(out_weight, column * local_channels, local_channels, 0)
    mixed = lax.psum_scatter(
        jnp.dot(conv_out, weight_rows, preferred_element_type=jnp.float32),
        "tp",
        scatter_dimension=0,
        tiled=True,
    )
    stream = residual.astype(jnp.float32) + lax.optimization_barrier(
        mixed.astype(jnp.bfloat16)
    ).astype(jnp.float32)
    normed = (
        stream * lax.rsqrt(jnp.mean(stream * stream, axis=-1, keepdims=True) + 1e-06) * ffn_gain
    ).astype(jnp.bfloat16)
    experts_n = lax.axis_size("sp")
    top_count = routes.shape[1]
    model_width = normed.shape[1]
    capacity = max(2, 2 * tok_dev * top_count // (columns * experts_n))
    slot_total = experts_n * capacity
    own_routes = lax.dynamic_slice_in_dim(routes, column * rows_own, rows_own, 0)
    own_weights = lax.dynamic_slice_in_dim(route_weights, column * rows_own, rows_own, 0)
    own_slots = slot_numbers(own_routes, capacity, experts_n)
    routing_table = dispatch_matrix(own_slots, slot_total)
    outgoing = jnp.dot(routing_table, normed, preferred_element_type=jnp.float32).astype(
        jnp.bfloat16
    )
    outgoing = outgoing.reshape(experts_n, capacity, model_width)
    arrived = lax.all_to_all(outgoing, "sp", split_axis=0, concat_axis=1, tiled=True).reshape(
        slot_total, model_width
    )
    gate_act = jnp.dot(arrived, whole_gate, preferred_element_type=jnp.float32)
    up_act = jnp.dot(arrived, whole_up, preferred_element_type=jnp.float32)
    hidden = (jax.nn.silu(gate_act) * up_act).astype(jnp.bfloat16)
    summed = jnp.dot(hidden, whole_down, preferred_element_type=jnp.float32)
    expert_out = summed.astype(jnp.bfloat16).reshape(experts_n, capacity, model_width)
    returned = lax.all_to_all(expert_out, "sp", split_axis=0, concat_axis=0, tiled=True).reshape(
        slot_total, model_width
    )
    combined = stream
    for member in range(top_count):
        chosen = jnp.take(returned, own_slots[:, member], axis=0).astype(jnp.float32)
        combined = combined + own_weights[:, member : member + 1] * chosen
    return combined.astype(jnp.bfloat16)


def solution(mesh):
    return jax.shard_map(
        shards,
        mesh=mesh,
        in_specs=(
            P(("sp", "tp"), None),
            P("sp", "tp"),
            P("sp", "tp"),
            P("sp"),
            P(None, "tp"),
            P("tp"),
            P("tp"),
            P(),
            P(),
            P("sp", None),
            P("sp", None),
            P("sp", None, "tp"),
            P("sp", None, "tp"),
            P("sp", "tp", None),
        ),
        out_specs=P(("sp", "tp"), None),
        check_vma=False,
    )
```

profile of v0, /device:TPU:0, one launch (start us, length us, event | category | flops | bytes accessed | tf_op | source)
XLA Modules:
  0.0 263.9 jit_solution(16011926092684907815)
XLA Ops:
  6.5 0.8 slice.300
  7.3 4.9 %collective-permute-start = (s32[30]{0:T(128)S(1)}, s32[30]{0:T(128)S(1)}, u32[]{:S(2)}, u32[]{:S(2)}) collective-permute-start(s32[30]{0:T(128)S(1)} %slice.300), channel_id=1, source_target_pairs={{0,4},{4,8},{8,12},{12,16},{16,20},{20,24},{24,28},{1,5},{5,9},{9,... | collective-permute-start | bytes 368 | tf_op jit(solution)/shard_map/ppermute | solution.py:13
  12.2 1.2 multiply_convert_fusion.4
  13.4 3.5 %collective-permute-start.1 = (bf16[30,256]{1,0:T(8,128)(2,1)S(1)}, bf16[30,256]{1,0:T(8,128)(2,1)S(1)}, u32[]{:S(2)}, u32[]{:S(2)}) collective-permute-start(bf16[30,256]{1,0:T(8,128)(2,1)S(1)} %slice.404), channel_id=1, source_target_pairs={{0,4},{4,8},{8,12},{12,16},{16,20},{20,24},{24,28},{1,5},{5,9},{9,... | collective-permute-start | bytes 46088 | tf_op jit(solution)/shard_map/ppermute | solution.py:13
  16.8 1.0 fusion.89
  17.9 1.0 fusion.90
  18.9 0.8 pad_add_fusion
  19.6 0.8 slice_compare_fusion.29
  20.4 0.8 slice_compare_fusion.28
  21.2 4.0 %fusion.17 = f32[512,256]{1,0:T(8,128)S(1)} fusion(f32[542,256]{1,0:T(8,128)S(1)} %maximum_convert_fusion, f32[256]{0:T(256)S(1)} %bitcast.119, f32[256]{0:T(256)S(1)} %bitcast.120, f32[256]{0:T(256)S(1)} %bitcast.91, f32[256]{0:T(256)S(1)} %bitcast.92, f32[256]{0:T(256)S(1)} %bitcast.93, f32[256]{0:T(256)S(1)} %bitcast.94, f32[256]{0:T(256)S(1)} %bitcast.95, ...), kind=kLoop, calls=%fused_computation.22 | loop fusion | flops 11927552 | bytes 16824320 | tf_op jit(solution)/shard_map/add | solution.py:63
  25.6 0.6 reduce_sum.38
  26.2 1.6 multiply_reduce_fusion.1
  28.5 0.6 sub.20
  29.1 4.0 %fusion.11 = f32[512,2048]{1,0:T(8,128)} fusion(bf16[1024,2048]{1,0:T(8,128)(2,1)} %param.23, s32[]{:T(128)S(6)} %select_n.136, f32[64,8,2,128]{3,2,1,0:T(2,128)S(1)} %bitcast.85, f32[512,256]{1,0:T(8,128)S(1)} %fusion.17, f32[64,8,2,128]{3,2,1,0:T(2,128)S(1)} %bitcast.86, f32[256]{0:T(256)S(1)} %copy-done.3, f32[256]{0:T(256)S(1)} %copy-done.4), kind=kOutput, calls=%fused_computation.15 | convolution fusion | flops 538050560 | bytes 6817796 | tf_op jit(solution)/shard_map/dot_general | solution.py:79
  33.2 0.7 all-gather.7.cloned.1.call-update
  33.9 0.7 all-gather.11.cloned.1.call-update
  36.9 41.2 %reduce-scatter.2.cloned.1.call-done = f32[128,2048]{1,0:T(8,128)} async-done(((f32[512,2048]{1,0:T(8,128)}), f32[128,2048]{1,0:T(8,128)}) %reduce-scatter.2.cloned.1.call-update) | async-done | bytes 1048592 | tf_op jit(solution)/shard_map/reduce_scatter | solution.py:78
  78.1 1.3 convert_element_type.59
  79.7 2.2 convolution_convert_fusion
  81.8 5.5 %all-to-all-start = ((bf16[8,64,2048]{2,1,0:T(8,128)(2,1)}), bf16[8,64,2048]{2,1,0:T(8,128)(2,1)S(1)}, u32[]{:S(2)}, u32[]{:S(2)}) async-start(bf16[8,64,2048]{2,1,0:T(8,128)(2,1)} %bitcast.34), calls=%async_computation.1 | async-start | bytes 4194304 | tf_op jit(solution)/shard_map/all_to_all | solution.py:103
  87.3 27.3 %all-gather.7.cloned.1.call-done = bf16[1,2048,1024]{2,1,0:T(8,128)(2,1)} async-done(((bf16[1,2048,256]{2,1,0:T(8,128)(2,1)}), bf16[1,2048,1024]{2,1,0:T(8,128)(2,1)}) %all-gather.7.cloned.1.call-update) | async-done | bytes 4194320 | tf_op jit(solution)/shard_map/all_gather | solution.py:48
  114.7 20.7 %all-to-all-done = bf16[8,64,2048]{2,1,0:T(8,128)(2,1)S(1)} async-done(((bf16[8,64,2048]{2,1,0:T(8,128)(2,1)}), bf16[8,64,2048]{2,1,0:T(8,128)(2,1)S(1)}, u32[]{:S(2)}, u32[]{:S(2)}) %all-to-all-start) | async-done | bytes 2097184 | tf_op jit(solution)/shard_map/all_to_all | solution.py:103
  135.4 6.0 %fusion.4 = f32[512,1024]{1,0:T(8,128)} fusion(bf16[512,2048]{1,0:T(8,128)(2,1)S(1)} %bitcast.88, bf16[1,2048,1024]{2,1,0:T(8,128)(2,1)} %all-gather.7.cloned.1.call-done), kind=kOutput, calls=%fused_computation.6 | convolution fusion | flops 2147483648 | bytes 8388608 | tf_op jit(solution)/shard_map/dot_general | solution.py:106
  141.4 9.4 %all-gather.11.cloned.1.call-done = bf16[1,1024,2048]{2,1,0:T(8,128)(2,1)} async-done(((bf16[1,256,2048]{2,1,0:T(8,128)(2,1)}), bf16[1,1024,2048]{2,1,0:T(8,128)(2,1)}) %all-gather.11.cloned.1.call-update) | async-done | bytes 4194320 | tf_op jit(solution)/shard_map/all_gather | solution.py:51
  150.8 36.4 %all-gather.9.cloned.1.call-done = bf16[1,2048,1024]{2,1,0:T(8,128)(2,1)} async-done(((bf16[1,2048,256]{2,1,0:T(8,128)(2,1)}), bf16[1,2048,1024]{2,1,0:T(8,128)(2,1)}) %all-gather.9.cloned.1.call-update) | async-done | bytes 4194320 | tf_op jit(solution)/shard_map/all_gather | solution.py:49
  187.2 10.0 %fusion.6 = bf16[512,2048]{1,0:T(8,128)(2,1)} fusion(bf16[1,1024,2048]{2,1,0:T(8,128)(2,1)} %all-gather.11.cloned.1.call-done, f32[512,1024]{1,0:T(8,128)} %fusion.4, bf16[512,2048]{1,0:T(8,128)(2,1)S(1)} %bitcast.89, bf16[1,2048,1024]{2,1,0:T(8,128)(2,1)} %all-gather.9.cloned.1.call-done), kind=kOutput, calls=%fused_computation.8 | convolution fusion | flops 4299161600 | bytes 14680064 | tf_op jit(solution)/shard_map/dot_general | solution.py:109
  197.2 5.5 %all-to-all-start.1 = ((bf16[8,64,2048]{2,1,0:T(8,128)(2,1)}), bf16[8,64,2048]{2,1,0:T(8,128)(2,1)S(1)}, u32[]{:S(2)}, u32[]{:S(2)}) async-start(bf16[8,64,2048]{2,1,0:T(8,128)(2,1)} %bitcast.87), calls=%async_computation.2 | async-start | bytes 4194304 | tf_op jit(solution)/shard_map/all_to_all | solution.py:111
  202.8 0.7 constant_dynamic-slice_fusion.1
  203.7 47.7 %all-to-all-done.1 = bf16[8,64,2048]{2,1,0:T(8,128)(2,1)S(1)} async-done(((bf16[8,64,2048]{2,1,0:T(8,128)(2,1)}), bf16[8,64,2048]{2,1,0:T(8,128)(2,1)S(1)}, u32[]{:S(2)}, u32[]{:S(2)}) %all-to-all-start.1) | async-done | bytes 2097184 | tf_op jit(solution)/shard_map/all_to_all | solution.py:111
  251.4 1.7 gather_fusion
  253.1 1.7 gather_fusion.1
  254.8 2.5 add_convert_fusion
  (46 shorter events, 3.8 us)
Async XLA Ops:
  6.5 28.7 %copy-start = (s32[512,2]{0,1:T(2,128)S(1)}, s32[512,2]{0,1:T(2,128)}, u32[]{:S(2)}) copy-start(s32[512,2]{0,1:T(2,128)} %param.25) | copy-start | bytes 12292
  6.5 71.6 %reduce-scatter.2.cloned.1.call-start = ((), (), s32[]{:S(2)}) async-start(), calls=%async_computation.3 | async-start | bytes 5242880 | tf_op jit(solution)/shard_map/reduce_scatter | solution.py:78
  7.3 11.5 %collective-permute-start = (s32[30]{0:T(128)S(1)}, s32[30]{0:T(128)S(1)}, u32[]{:S(2)}, u32[]{:S(2)}) collective-permute-start(s32[30]{0:T(128)S(1)} %slice.300), channel_id=1, source_target_pairs={{0,4},{4,8},{8,12},{12,16},{16,20},{20,24},{24,28},{1,5},{5,9},{9,... | collective-permute-start | bytes 368 | tf_op jit(solution)/shard_map/ppermute | solution.py:13
  13.4 7.8 %collective-permute-start.1 = (bf16[30,256]{1,0:T(8,128)(2,1)S(1)}, bf16[30,256]{1,0:T(8,128)(2,1)S(1)}, u32[]{:S(2)}, u32[]{:S(2)}) collective-permute-start(bf16[30,256]{1,0:T(8,128)(2,1)S(1)} %slice.404), channel_id=1, source_target_pairs={{0,4},{4,8},{8,12},{12,16},{16,20},{20,24},{24,28},{1,5},{5,9},{9,... | collective-permute-start | bytes 46088 | tf_op jit(solution)/shard_map/ppermute | solution.py:13
  25.6 3.5 %copy-start.3 = (f32[256]{0:T(256)S(1)}, f32[256]{0:T(256)}, u32[]{:S(2)}) copy-start(f32[256]{0:T(256)} %param.22) | copy-start | bytes 3076
  25.6 3.5 %copy-start.4 = (f32[256]{0:T(256)S(1)}, f32[256]{0:T(256)}, u32[]{:S(2)}) copy-start(f32[256]{0:T(256)} %param.21) | copy-start | bytes 3076
  33.1 81.6 %all-gather.7.cloned.1.call-start = ((), (), s32[]{:S(2)}) async-start(), calls=%async_computation.4 | async-start | bytes 5242880 | tf_op jit(solution)/shard_map/all_gather | solution.py:48
  33.9 45.5 %copy-start.1 = (bf16[128,2048]{1,0:T(8,128)(2,1)S(1)}, bf16[128,2048]{1,0:T(8,128)(2,1)}, u32[]{:S(2)}) copy-start(bf16[128,2048]{1,0:T(8,128)(2,1)} %param.16) | copy-start | bytes 1572868
  33.9 116.9 %all-gather.11.cloned.1.call-start = ((), (), s32[]{:S(2)}) async-start(), calls=%async_computation.6 | async-start | bytes 5242880 | tf_op jit(solution)/shard_map/all_gather | solution.py:51
  34.6 45.0 %copy-start.2 = (f32[2048]{0:T(1024)S(1)}, f32[2048]{0:T(1024)}, u32[]{:S(2)}) copy-start(f32[2048]{0:T(1024)} %param.24) | copy-start | bytes 24580
  34.6 152.6 %all-gather.9.cloned.1.call-start = ((), (), s32[]{:S(2)}) async-start(), calls=%async_computation.5 | async-start | bytes 5242880 | tf_op jit(solution)/shard_map/all_gather | solution.py:49
  81.8 53.6 %all-to-all-start = ((bf16[8,64,2048]{2,1,0:T(8,128)(2,1)}), bf16[8,64,2048]{2,1,0:T(8,128)(2,1)S(1)}, u32[]{:S(2)}, u32[]{:S(2)}) async-start(bf16[8,64,2048]{2,1,0:T(8,128)(2,1)} %bitcast.34), calls=%async_computation.1 | async-start | bytes 4194304 | tf_op jit(solution)/shard_map/all_to_all | solution.py:103
  197.2 54.2 %all-to-all-start.1 = ((bf16[8,64,2048]{2,1,0:T(8,128)(2,1)}), bf16[8,64,2048]{2,1,0:T(8,128)(2,1)S(1)}, u32[]{:S(2)}, u32[]{:S(2)}) async-start(bf16[8,64,2048]{2,1,0:T(8,128)(2,1)} %bitcast.87), calls=%async_computation.2 | async-start | bytes 4194304 | tf_op jit(solution)/shard_map/all_to_all | solution.py:111
Sparse Core Ops, SparseCore 0:
  33.2 44.8 reduce-scatter.1
  79.7 34.9 all-gather.6
  116.3 34.4 all-gather.10
  152.2 34.9 all-gather.8
where the time goes:
time: 265 us; the launch traced here: 264 us
  waiting for transfers between devices  185 us (70%)
  matrix products  22.1 us (8%)
  starting transfers between devices  19.5 us (7%)
  other arithmetic  14.7 us (6%)
  between operations  13.4 us (5%)
  local copies, waits for them, and re-layouts  9.39 us (4%)
    all_to_all x1, waiting for transfers between devices, shards(): lax.all_to_all(expert_out, 'sp', split_axis=0, concat_axis=0, tiled=True)  47.7 us
    reduce_scatter x1, waiting for transfers between devices, shards(): lax.psum_scatter(jnp.dot(conv_out, weight_rows, preferred_element_type=jn...  41.2 us
    all_gather x1, waiting for transfers between devices, shards(): lax.all_gather(w_up[0], 'tp', axis=1, tiled=True)  36.4 us
    all_gather x1, waiting for transfers between devices, shards(): lax.all_gather(w_gate[0], 'tp', axis=1, tiled=True)  27.3 us
    all_to_all x1, waiting for transfers between devices, shards(): lax.all_to_all(outgoing, 'sp', split_axis=0, concat_axis=1, tiled=True)  20.7 us
    dot_general x1, matrix products, shards(): summed = jnp.dot(hidden, whole_down, preferred_element_type=jnp.float32)  10 us
    all_gather x1, waiting for transfers between devices, shards(): whole_down = lax.all_gather(w_down[0], 'tp', axis=0, tiled=True)  9.38 us
    ppermute x2, starting transfers between devices, passed_along(): lax.ppermute(value, axis, [(source, source + steps) for source in range(i...  8.32 us
  transfers between devices with their start and end apart: 8, of which 6 were waited for; matrix products, arithmetic and copies ran while one was open for 7% of the time, Pallas kernels for 0%

commit v1 on v0

--- a/solution.py
+++ b/solution.py
@@ -5,6 +5,29 @@
 
 DC = 1024
 CONV_GROUPS = 8
+
+
+def cut_along(array, dim, size):
+    lengths = array.shape
+    blocks = array.reshape(*lengths[:dim], size, lengths[dim] // size, *lengths[dim + 1 :])
+    return jnp.moveaxis(blocks, dim, 0)
+
+
+def in_order(pieces, dim):
+    dims = list(pieces.shape[1:])
+    dims[dim] *= pieces.shape[0]
+    return jnp.moveaxis(pieces, 0, dim).reshape(dims)
+
+
+def pairwise_exchange(x, axis, split_dim, concat_dim):
+    size, index = (lax.axis_size(axis), lax.axis_index(axis))
+    blocks = cut_along(x, split_dim, size)
+    outs = [blocks[index]]
+    for step in range(1, size):
+        sent = blocks[index ^ step]
+        outs.append(lax.ppermute(sent, axis, [(i, i ^ step) for i in range(size)]))
+    blocks = jnp.stack(outs)[index ^ jnp.arange(size)]
+    return in_order(blocks, concat_dim)
 
 
 def passed_along(value, axis, steps):
@@ -108,9 +131,7 @@
     hidden = (jax.nn.silu(gate_act) * up_act).astype(jnp.bfloat16)
     summed = jnp.dot(hidden, whole_down, preferred_element_type=jnp.float32)
     expert_out = summed.astype(jnp.bfloat16).reshape(experts_n, capacity, model_width)
-    returned = lax.all_to_all(expert_out, "sp", split_axis=0, concat_axis=0, tiled=True).reshape(
-        slot_total, model_width
-    )
+    returned = pairwise_exchange(expert_out, "sp", 0, 0).reshape(slot_total, model_width)
     combined = stream
     for member in range(top_count):
         chosen = jnp.take(returned, own_slots[:, member], axis=0).astype(jnp.float32)

time: 265 us -> 265 us (level)
  the two profiles are of different devices: /device:TPU:0 before, /device:TPU:16 now
where the time goes in v1:
time: 265 us; the launch traced here: 264 us
  waiting for transfers between devices  179 us (68%)
  matrix products  22 us (8%)
  starting transfers between devices  21.4 us (8%)
  other arithmetic  14.7 us (6%)
  between operations  13.5 us (5%)
  local copies, waits for them, and re-layouts  13.4 us (5%)
    ppermute x7, waiting for transfers between devices, pairwise_exchange(): outs.append(lax.ppermute(sent, axis, [(i, i ^ step) for i in range(size)]))  43.8 us
    reduce_scatter x1, waiting for transfers between devices, shards(): lax.psum_scatter(jnp.dot(conv_out, weight_rows, preferred_element_type=jn...  41 us
    all_gather x1, waiting for transfers between devices, shards(): lax.all_gather(w_up[0], 'tp', axis=1, tiled=True)  36.4 us
    all_gather x1, waiting for transfers between devices, shards(): lax.all_gather(w_gate[0], 'tp', axis=1, tiled=True)  26.6 us
    all_to_all x1, waiting for transfers between devices, shards(): lax.all_to_all(outgoing, 'sp', split_axis=0, concat_axis=1, tiled=True)  17.9 us
    all_gather x1, waiting for transfers between devices, shards(): whole_down = lax.all_gather(w_down[0], 'tp', axis=0, tiled=True)  11.5 us
    dot_general x1, matrix products, shards(): summed = jnp.dot(hidden, whole_down, preferred_element_type=jnp.float32)  9.23 us
    ppermute x7, starting transfers between devices, pairwise_exchange(): outs.append(lax.ppermute(sent, axis, [(i, i ^ step) for i in range(size)]))  8.42 us
  transfers between devices with their start and end apart: 14, of which 11 were waited for; matrix products, arithmetic and copies ran while one was open for 7% of the time, Pallas kernels for 0%

profile of v1, /device:TPU:16, one launch (start us, length us, event | category | flops | bytes accessed | tf_op | source)
XLA Modules:
  0.0 264.2 jit_solution(16331051741013565432)
XLA Ops:
  7.3 3.4 %collective-permute-start = (s32[30]{0:T(128)S(1)}, s32[30]{0:T(128)S(1)}, u32[]{:S(2)}, u32[]{:S(2)}) collective-permute-start(s32[30]{0:T(128)S(1)} %slice.300), channel_id=1, source_target_pairs={{0,4},{4,8},{8,12},{12,16},{16,20},{20,24},{24,28},{1,5},{5,9},{9,... | collective-permute-start | bytes 368 | tf_op jit(solution)/shard_map/ppermute | solution.py:36
  10.7 1.2 multiply_convert_fusion.4
  11.9 3.5 %collective-permute-start.1 = (bf16[30,256]{1,0:T(8,128)(2,1)S(1)}, bf16[30,256]{1,0:T(8,128)(2,1)S(1)}, u32[]{:S(2)}, u32[]{:S(2)}) collective-permute-start(bf16[30,256]{1,0:T(8,128)(2,1)S(1)} %slice.406), channel_id=1, source_target_pairs={{0,4},{4,8},{8,12},{12,16},{16,20},{20,24},{24,28},{1,5},{5,9},{9,... | collective-permute-start | bytes 46088 | tf_op jit(solution)/shard_map/ppermute | solution.py:36
  15.4 1.0 fusion.90
  16.4 1.0 fusion.91
  18.1 0.8 slice_compare_fusion.29
  19.8 4.0 %fusion.17 = f32[512,256]{1,0:T(8,128)S(1)} fusion(f32[542,256]{1,0:T(8,128)S(1)} %maximum_convert_fusion, f32[256]{0:T(256)S(1)} %bitcast.151, f32[256]{0:T(256)S(1)} %bitcast.152, f32[256]{0:T(256)S(1)} %bitcast.123, f32[256]{0:T(256)S(1)} %bitcast.124, f32[256]{0:T(256)S(1)} %bitcast.125, f32[256]{0:T(256)S(1)} %bitcast.126, f32[256]{0:T(256)S(1)} %bitcast.127, ...), kind=kLoop, calls=%fused_computation.23 | loop fusion | flops 11927552 | bytes 16824320 | tf_op jit(solution)/shard_map/add | solution.py:86
  24.8 1.6 multiply_reduce_fusion.1
  27.7 4.0 %fusion.11 = f32[512,2048]{1,0:T(8,128)} fusion(bf16[1024,2048]{1,0:T(8,128)(2,1)} %param.23, s32[]{:T(128)S(6)} %select_n.170, f32[64,8,2,128]{3,2,1,0:T(2,128)S(1)} %bitcast.116, f32[512,256]{1,0:T(8,128)S(1)} %fusion.17, f32[64,8,2,128]{3,2,1,0:T(2,128)S(1)} %bitcast.117, f32[256]{0:T(256)S(1)} %copy-done.5, f32[256]{0:T(256)S(1)} %copy-done.6), kind=kOutput, calls=%fused_computation.16 | convolution fusion | flops 538050560 | bytes 6817796 | tf_op jit(solution)/shard_map/dot_general | solution.py:102
  35.4 41.0 %reduce-scatter.2.cloned.1.call-done = f32[128,2048]{1,0:T(8,128)} async-done(((f32[512,2048]{1,0:T(8,128)}), f32[128,2048]{1,0:T(8,128)}) %reduce-scatter.2.cloned.1.call-update) | async-done | bytes 1048592 | tf_op jit(solution)/shard_map/reduce_scatter | solution.py:101
  76.4 1.3 convert_element_type.59
  78.0 2.1 convolution_convert_fusion
  80.1 6.0 %all-to-all-start = ((bf16[8,64,2048]{2,1,0:T(8,128)(2,1)}), bf16[8,64,2048]{2,1,0:T(8,128)(2,1)S(1)}, u32[]{:S(2)}, u32[]{:S(2)}) async-start(bf16[8,64,2048]{2,1,0:T(8,128)(2,1)} %bitcast.34), calls=%async_computation.1 | async-start | bytes 4194304 | tf_op jit(solution)/shard_map/all_to_all | solution.py:126
  86.4 26.6 %all-gather.7.cloned.1.call-done = bf16[1,2048,1024]{2,1,0:T(8,128)(2,1)} async-done(((bf16[1,2048,256]{2,1,0:T(8,128)(2,1)}), bf16[1,2048,1024]{2,1,0:T(8,128)(2,1)}) %all-gather.7.cloned.1.call-update) | async-done | bytes 4194320 | tf_op jit(solution)/shard_map/all_gather | solution.py:71
  113.0 17.9 %all-to-all-done = bf16[8,64,2048]{2,1,0:T(8,128)(2,1)S(1)} async-done(((bf16[8,64,2048]{2,1,0:T(8,128)(2,1)}), bf16[8,64,2048]{2,1,0:T(8,128)(2,1)S(1)}, u32[]{:S(2)}, u32[]{:S(2)}) %all-to-all-start) | async-done | bytes 2097184 | tf_op jit(solution)/shard_map/all_to_all | solution.py:126
  131.0 6.7 %fusion.4 = f32[512,1024]{1,0:T(8,128)} fusion(bf16[512,2048]{1,0:T(8,128)(2,1)S(1)} %bitcast.120, bf16[1,2048,1024]{2,1,0:T(8,128)(2,1)} %all-gather.7.cloned.1.call-done), kind=kOutput, calls=%fused_computation.7 | convolution fusion | flops 2147483648 | bytes 8388608 | tf_op jit(solution)/shard_map/dot_general | solution.py:129
  137.6 11.5 %all-gather.11.cloned.1.call-done = bf16[1,1024,2048]{2,1,0:T(8,128)(2,1)} async-done(((bf16[1,256,2048]{2,1,0:T(8,128)(2,1)}), bf16[1,1024,2048]{2,1,0:T(8,128)(2,1)}) %all-gather.11.cloned.1.call-update) | async-done | bytes 4194320 | tf_op jit(solution)/shard_map/all_gather | solution.py:74
  149.1 36.4 %all-gather.9.cloned.1.call-done = bf16[1,2048,1024]{2,1,0:T(8,128)(2,1)} async-done(((bf16[1,2048,256]{2,1,0:T(8,128)(2,1)}), bf16[1,2048,1024]{2,1,0:T(8,128)(2,1)}) %all-gather.9.cloned.1.call-update) | async-done | bytes 4194320 | tf_op jit(solution)/shard_map/all_gather | solution.py:72
  185.5 9.2 %fusion.6 = bf16[512,2048]{1,0:T(8,128)(2,1)S(1)} fusion(bf16[1,1024,2048]{2,1,0:T(8,128)(2,1)} %all-gather.11.cloned.1.call-done, f32[512,1024]{1,0:T(8,128)} %fusion.4, bf16[512,2048]{1,0:T(8,128)(2,1)} %bitcast.121, bf16[1,2048,1024]{2,1,0:T(8,128)(2,1)} %all-gather.9.cloned.1.call-done), kind=kOutput, calls=%fused_computation.9 | convolution fusion | flops 4299161600 | bytes 14680064 | tf_op jit(solution)/shard_map/dot_general | solution.py:132
  195.0 1.5 collective-permute-start.2
  197.2 1.5 collective-permute-start.3
  199.8 3.3 %collective-permute-start.6 = (bf16[1,64,2048]{2,1,0:T(8,128)(2,1)S(1)}, bf16[1,64,2048]{2,1,0:T(8,128)(2,1)S(1)}, u32[]{:S(2)}, u32[]{:S(2)}) collective-permute-start(bf16[1,64,2048]{2,1,0:T(8,128)(2,1)S(1)} %get-tuple-element.10), channel_id=1, source_target_pairs={{0,20},{4,16},{8,28},{12,24},{16,4},{20,0},{24,12},{28,8},{1,21},{... | collective-permute-start | bytes 786440 | tf_op jit(solution)/shard_map/ppermute | solution.py:28
  204.1 10.2 %collective-permute-done.3 = bf16[1,64,2048]{2,1,0:T(8,128)(2,1)S(1)} collective-permute-done((bf16[1,64,2048]{2,1,0:T(8,128)(2,1)S(1)}, bf16[1,64,2048]{2,1,0:T(8,128)(2,1)S(1)}, u32[]{:S(2)}, u32[]{:S(2)}) %collective-permute-start.3) | collective-permute-done | bytes 262176 | tf_op jit(solution)/shard_map/ppermute | solution.py:28
  214.8 4.1 %collective-permute-done.4 = bf16[1,64,2048]{2,1,0:T(8,128)(2,1)S(1)} collective-permute-done((bf16[1,64,2048]{2,1,0:T(8,128)(2,1)S(1)}, bf16[1,64,2048]{2,1,0:T(8,128)(2,1)S(1)}, u32[]{:S(2)}, u32[]{:S(2)}) %collective-permute-start.4) | collective-permute-done | bytes 262176 | tf_op jit(solution)/shard_map/ppermute | solution.py:28
  219.0 15.6 %collective-permute-done.6 = bf16[1,64,2048]{2,1,0:T(8,128)(2,1)S(1)} collective-permute-done((bf16[1,64,2048]{2,1,0:T(8,128)(2,1)S(1)}, bf16[1,64,2048]{2,1,0:T(8,128)(2,1)S(1)}, u32[]{:S(2)}, u32[]{:S(2)}) %collective-permute-start.6) | collective-permute-done | bytes 262176 | tf_op jit(solution)/shard_map/ppermute | solution.py:28
  234.6 8.5 %collective-permute-done.7 = bf16[1,64,2048]{2,1,0:T(8,128)(2,1)S(1)} collective-permute-done((bf16[1,64,2048]{2,1,0:T(8,128)(2,1)S(1)}, bf16[1,64,2048]{2,1,0:T(8,128)(2,1)S(1)}, u32[]{:S(2)}, u32[]{:S(2)}) %collective-permute-start.7) | collective-permute-done | bytes 262176 | tf_op jit(solution)/shard_map/ppermute | solution.py:28
  243.1 5.0 %collective-permute-done.8 = bf16[1,64,2048]{2,1,0:T(8,128)(2,1)S(1)} collective-permute-done((bf16[1,64,2048]{2,1,0:T(8,128)(2,1)S(1)}, bf16[1,64,2048]{2,1,0:T(8,128)(2,1)S(1)}, u32[]{:S(2)}, u32[]{:S(2)}) %collective-permute-start.8) | collective-permute-done | bytes 262176 | tf_op jit(solution)/shard_map/ppermute | solution.py:28
  248.1 1.3 copy-done.2
  249.4 2.3 gather_fusion
  251.7 1.7 gather_fusion.1
  253.4 1.7 gather_fusion.2
  255.2 2.5 add_convert_fusion
  (73 shorter events, 12.3 us)
Async XLA Ops:
  6.5 27.2 %copy-start = (s32[512,2]{0,1:T(2,128)S(1)}, s32[512,2]{0,1:T(2,128)}, u32[]{:S(2)}) copy-start(s32[512,2]{0,1:T(2,128)} %param.25) | copy-start | bytes 12292
  6.5 69.9 %reduce-scatter.2.cloned.1.call-start = ((), (), s32[]{:S(2)}) async-start(), calls=%async_computation.2 | async-start | bytes 5242880 | tf_op jit(solution)/shard_map/reduce_scatter | solution.py:101
  7.3 10.1 %collective-permute-start = (s32[30]{0:T(128)S(1)}, s32[30]{0:T(128)S(1)}, u32[]{:S(2)}, u32[]{:S(2)}) collective-permute-start(s32[30]{0:T(128)S(1)} %slice.300), channel_id=1, source_target_pairs={{0,4},{4,8},{8,12},{12,16},{16,20},{20,24},{24,28},{1,5},{5,9},{9,... | collective-permute-start | bytes 368 | tf_op jit(solution)/shard_map/ppermute | solution.py:36
  11.9 7.8 %collective-permute-start.1 = (bf16[30,256]{1,0:T(8,128)(2,1)S(1)}, bf16[30,256]{1,0:T(8,128)(2,1)S(1)}, u32[]{:S(2)}, u32[]{:S(2)}) collective-permute-start(bf16[30,256]{1,0:T(8,128)(2,1)S(1)} %slice.406), channel_id=1, source_target_pairs={{0,4},{4,8},{8,12},{12,16},{16,20},{20,24},{24,28},{1,5},{5,9},{9,... | collective-permute-start | bytes 46088 | tf_op jit(solution)/shard_map/ppermute | solution.py:36
  24.1 3.5 %copy-start.5 = (f32[256]{0:T(256)S(1)}, f32[256]{0:T(256)}, u32[]{:S(2)}) copy-start(f32[256]{0:T(256)} %param.22) | copy-start | bytes 3076
  24.1 3.5 %copy-start.6 = (f32[256]{0:T(256)S(1)}, f32[256]{0:T(256)}, u32[]{:S(2)}) copy-start(f32[256]{0:T(256)} %param.21) | copy-start | bytes 3076
  31.6 81.4 %all-gather.7.cloned.1.call-start = ((), (), s32[]{:S(2)}) async-start(), calls=%async_computation.3 | async-start | bytes 5242880 | tf_op jit(solution)/shard_map/all_gather | solution.py:71
  32.4 45.3 %copy-start.1 = (bf16[128,2048]{1,0:T(8,128)(2,1)S(1)}, bf16[128,2048]{1,0:T(8,128)(2,1)}, u32[]{:S(2)}) copy-start(bf16[128,2048]{1,0:T(8,128)(2,1)} %param.16) | copy-start | bytes 1572868
  32.4 116.7 %all-gather.11.cloned.1.call-start = ((), (), s32[]{:S(2)}) async-start(), calls=%async_computation.5 | async-start | bytes 5242880 | tf_op jit(solution)/shard_map/all_gather | solution.py:74
  33.1 44.9 %copy-start.4 = (f32[2048]{0:T(1024)S(1)}, f32[2048]{0:T(1024)}, u32[]{:S(2)}) copy-start(f32[2048]{0:T(1024)} %param.24) | copy-start | bytes 24580
  33.1 152.4 %all-gather.9.cloned.1.call-start = ((), (), s32[]{:S(2)}) async-start(), calls=%async_computation.4 | async-start | bytes 5242880 | tf_op jit(solution)/shard_map/all_gather | solution.py:72
  80.1 50.8 %all-to-all-start = ((bf16[8,64,2048]{2,1,0:T(8,128)(2,1)}), bf16[8,64,2048]{2,1,0:T(8,128)(2,1)S(1)}, u32[]{:S(2)}, u32[]{:S(2)}) async-start(bf16[8,64,2048]{2,1,0:T(8,128)(2,1)} %bitcast.34), calls=%async_computation.1 | async-start | bytes 4194304 | tf_op jit(solution)/shard_map/all_to_all | solution.py:126
  130.9 6.7 %copy-start.3 = (bf16[8,64,2048]{2,1,0:T(8,128)(2,1)}, bf16[8,64,2048]{2,1,0:T(8,128)(2,1)S(1)}, u32[]{:S(2)}) copy-start(bf16[8,64,2048]{2,1,0:T(8,128)(2,1)S(1)} %all-to-all-done) | copy-start | bytes 6291460
  195.0 8.5 %collective-permute-start.2 = (bf16[1,64,2048]{2,1,0:T(8,128)(2,1)S(1)}, bf16[1,64,2048]{2,1,0:T(8,128)(2,1)S(1)}, u32[]{:S(2)}, u32[]{:S(2)}) collective-permute-start(bf16[1,64,2048]{2,1,0:T(8,128)(2,1)S(1)} %get-tuple-element.14), channel_id=1, source_target_pairs={{0,4},{4,0},{8,12},{12,8},{16,20},{20,16},{24,28},{28,24},{1,5},{5... | collective-permute-start | bytes 786440 | tf_op jit(solution)/shard_map/ppermute | solution.py:28
  197.2 17.1 %collective-permute-start.3 = (bf16[1,64,2048]{2,1,0:T(8,128)(2,1)S(1)}, bf16[1,64,2048]{2,1,0:T(8,128)(2,1)S(1)}, u32[]{:S(2)}, u32[]{:S(2)}) collective-permute-start(bf16[1,64,2048]{2,1,0:T(8,128)(2,1)S(1)} %get-tuple-element.13), channel_id=1, source_target_pairs={{0,8},{4,12},{8,0},{12,4},{16,24},{20,28},{24,16},{28,20},{1,9},{5... | collective-permute-start | bytes 786440 | tf_op jit(solution)/shard_map/ppermute | solution.py:28
  198.7 20.2 %collective-permute-start.4 = (bf16[1,64,2048]{2,1,0:T(8,128)(2,1)S(1)}, bf16[1,64,2048]{2,1,0:T(8,128)(2,1)S(1)}, u32[]{:S(2)}, u32[]{:S(2)}) collective-permute-start(bf16[1,64,2048]{2,1,0:T(8,128)(2,1)S(1)} %get-tuple-element.12), channel_id=1, source_target_pairs={{0,12},{4,8},{8,4},{12,0},{16,28},{20,24},{24,20},{28,16},{1,13},{... | collective-permute-start | bytes 786440 | tf_op jit(solution)/shard_map/ppermute | solution.py:28
  199.2 19.7 %collective-permute-start.5 = (bf16[1,64,2048]{2,1,0:T(8,128)(2,1)S(1)}, bf16[1,64,2048]{2,1,0:T(8,128)(2,1)S(1)}, u32[]{:S(2)}, u32[]{:S(2)}) collective-permute-start(bf16[1,64,2048]{2,1,0:T(8,128)(2,1)S(1)} %get-tuple-element.11), channel_id=1, source_target_pairs={{0,16},{4,20},{8,24},{12,28},{16,0},{20,4},{24,8},{28,12},{1,17},{... | collective-permute-start | bytes 786440 | tf_op jit(solution)/shard_map/ppermute | solution.py:28
  199.8 34.8 %collective-permute-start.6 = (bf16[1,64,2048]{2,1,0:T(8,128)(2,1)S(1)}, bf16[1,64,2048]{2,1,0:T(8,128)(2,1)S(1)}, u32[]{:S(2)}, u32[]{:S(2)}) collective-permute-start(bf16[1,64,2048]{2,1,0:T(8,128)(2,1)S(1)} %get-tuple-element.10), channel_id=1, source_target_pairs={{0,20},{4,16},{8,28},{12,24},{16,4},{20,0},{24,12},{28,8},{1,21},{... | collective-permute-start | bytes 786440 | tf_op jit(solution)/shard_map/ppermute | solution.py:28
  203.5 39.5 %collective-permute-start.7 = (bf16[1,64,2048]{2,1,0:T(8,128)(2,1)S(1)}, bf16[1,64,2048]{2,1,0:T(8,128)(2,1)S(1)}, u32[]{:S(2)}, u32[]{:S(2)}) collective-permute-start(bf16[1,64,2048]{2,1,0:T(8,128)(2,1)S(1)} %get-tuple-element.9), channel_id=1, source_target_pairs={{0,24},{4,28},{8,16},{12,20},{16,8},{20,12},{24,0},{28,4},{1,25},{... | collective-permute-start | bytes 786440 | tf_op jit(solution)/shard_map/ppermute | solution.py:28
  214.3 33.8 %collective-permute-start.8 = (bf16[1,64,2048]{2,1,0:T(8,128)(2,1)S(1)}, bf16[1,64,2048]{2,1,0:T(8,128)(2,1)S(1)}, u32[]{:S(2)}, u32[]{:S(2)}) collective-permute-start(bf16[1,64,2048]{2,1,0:T(8,128)(2,1)S(1)} %get-tuple-element.8), channel_id=1, source_target_pairs={{0,28},{4,24},{8,20},{12,16},{16,12},{20,8},{24,4},{28,0},{1,29},{... | collective-permute-start | bytes 786440 | tf_op jit(solution)/shard_map/ppermute | solution.py:28
  248.1 1.4 copy-start.2
Sparse Core Ops, SparseCore 0:
  31.8 44.6 reduce-scatter.1
  78.0 35.0 all-gather.6
  114.6 34.4 all-gather.10
  150.5 34.9 all-gather.8
